TPU v7x, 32 devices: a whole 2x2x4 slice. The times are simulated.
32 devices in a mesh: rep: 4 (over z), fs: 4 (over y, x), tp: 2 (over core).
Axes of the slice: x: 2, y: 2, z: 4, core: 2. Of those that a mesh axis runs over, the one named last changes fastest.
Arguments:
- inputs: bfloat16 [512, 2048], P(('rep', 'fs', 'tp')), may hold values from -6 to 6
- cotangent: bfloat16 [512, 2048], P(('rep', 'fs', 'tp')), may hold values from -6 to 6
- norm_gain: float32 [2048], replicated, may hold values from 0.1 to 1.9
- gate_weight: bfloat16 [2048, 2816], P(None, ('fs', 'tp')), may hold values from -0.125 to 0.125
- up_weight: bfloat16 [2048, 2816], P(None, ('fs', 'tp')), may hold values from -0.125 to 0.125
- down_weight: bfloat16 [2816, 2048], P(('fs', 'tp')), may hold values from -0.109375 to 0.109375
Outputs:
- input_grad: bfloat16 [512, 2048], P(('rep', 'fs', 'tp'))
- gain_grad: float32 [2048], replicated
- down_grad: float32 [2816, 2048], P(('fs', 'tp'), 'rep')
All inputs are finite; a program needn't handle non-finite values.
Results may differ from a plain program's by a relative error of at most 0.0066.
Values may be sent and summed in bfloat16 or wider, within the bound.
A program may use at most 64 MiB of HBM per device.

v0:
```python
import jax
import jax.numpy as jnp
from jax import lax
from jax.sharding import PartitionSpec as P

EPS = 1e-06


def across_tokens(left, right):
    return lax.dot_general(
        left, right, (((0,), (0,)), ((), ())), preferred_element_type=jnp.float32
    )


def across_columns(left, right):
    return lax.dot_general(
        left, right, (((1,), (1,)), ((), ())), preferred_element_type=jnp.float32
    )


def per_device(inputs, cotangent, norm_gain, gate_weight, up_weight, down_weight):
    whole_x, whole_dy = (
        lax.all_gather(inputs, ("fs", "tp"), axis=0, tiled=True),
        lax.all_gather(cotangent, ("fs", "tp"), axis=0, tiled=True),
    )
    xf = whole_x.astype(jnp.float32)
    inv = lax.rsqrt(jnp.mean(xf * xf, axis=-1, keepdims=True) + EPS)
    normed = xf * inv
    hidden_in = (normed * norm_gain).astype(jnp.bfloat16)
    gate = jnp.dot(hidden_in, gate_weight, preferred_element_type=jnp.float32)
    up = jnp.dot(hidden_in, up_weight, preferred_element_type=jnp.float32)
    sig = jax.nn.sigmoid(gate)
    act = gate * sig
    hidden = (act * up).astype(jnp.bfloat16)
    d_hidden = 0.5 * across_columns(whole_dy, down_weight)
    d_gate = (d_hidden * up * sig * (1.0 + gate * (1.0 - sig))).astype(jnp.bfloat16)
    d_up = (d_hidden * act).astype(jnp.bfloat16)
    own_rows = inputs.shape[0]
    d_in = lax.psum_scatter(
        across_columns(d_gate, gate_weight) + across_columns(d_up, up_weight),
        ("fs", "tp"),
        scatter_dimension=0,
        tiled=True,
    )
    offset = lax.axis_index(("fs", "tp")) * own_rows
    own_normed = lax.dynamic_slice_in_dim(normed, offset, own_rows, 0)
    own_inv = lax.dynamic_slice_in_dim(inv, offset, own_rows, 0)
    gain_grad = lax.psum(jnp.sum(d_in * own_normed, axis=0), ("rep", "fs", "tp"))
    scaled = d_in * norm_gain
    input_grad = (
        own_inv * (scaled - own_normed * jnp.mean(scaled * own_normed, axis=-1, keepdims=True))
    ).astype(jnp.bfloat16)
    input_grad, gain_grad = (input_grad, gain_grad)
    part_down = 0.5 * across_tokens(whole_dy, hidden)
    got_down = lax.all_to_all(
        part_down[None].astype(jnp.bfloat16), "rep", split_axis=1, concat_axis=0, tiled=True
    ).astype(jnp.float32)
    down_grad = jnp.sum(got_down, axis=0).T
    return (input_grad, gain_grad, down_grad)


def solution(mesh):
    return jax.shard_map(
        per_device,
        mesh=mesh,
        in_specs=(
            P(("rep", "fs", "tp"), None),
            P(("rep", "fs", "tp"), None),
            P(),
            P(None, ("fs", "tp")),
            P(None, ("fs", "tp")),
            P(("fs", "tp"), None),
        ),
        out_specs=(P(("rep", "fs", "tp"), None), P(), P(("fs", "tp"), "rep")),
        check_vma=False,
    )
```

profile of v0, /device:TPU:0, one launch (start us, length us, event | category | flops | bytes accessed | tf_op | source)
XLA Modules:
  0.0 166.7 jit_solution(2304956729085242355)
XLA Ops:
  7.2 11.8 %all_gather.6 = bf16[128,2048]{1,0:T(8,128)(2,1)S(1)} all-gather(bf16[16,2048]{1,0:T(8,128)(2,1)} %param.6), channel_id=1, replica_groups=mesh['rep'=4,'fs'=4,'tp'=2] {'fs','tp'}, dimensions={0}, use_global_device_ids=true | all-gather | bytes 589824 | tf_op jit(solution)/shard_map/all_gather | solution.py:23
  19.0 0.2 fusion.2
  19.2 1.4 fusion.3
  20.7 0.6 fusion.4
  21.3 0.3 copy-done.6
  21.6 9.5 %all_gather.7 = bf16[128,2048]{1,0:T(8,128)(2,1)S(1)} all-gather(bf16[16,2048]{1,0:T(8,128)(2,1)S(1)} %copy-done.6), channel_id=1, replica_groups=mesh['rep'=4,'fs'=4,'tp'=2] {'fs','tp'}, dimensions={0}, use_global_device_ids=true | all-gather | bytes 589824 | tf_op jit(solution)/shard_map/all_gather | solution.py:24
  31.1 0.8 copy-done.1
  31.9 0.5 convolution_multiply_fusion.1
  32.4 0.5 fusion.6
  33.0 1.5 convolution_add_fusion
  34.5 1.8 %fusion.1 = bf16[1,2048,352]{1,2,0:T(8,128)(2,1)S(1)} fusion(bf16[128,2048]{1,0:T(8,128)(2,1)} %copy-done.1, f32[128,352]{0,1:T(8,128)} %copy-done.5, f32[128,352]{0,1:T(8,128)} %copy-done.2), kind=kOutput, calls=%fused_computation.2 | convolution fusion | flops 186261504 | bytes 2326528 | tf_op jit(solution)/shard_map/dot_general | solution.py:10
  36.3 5.7 %copy.12 = bf16[1,2048,352]{2,0,1:T(2,128)(2,1)} copy(bf16[1,2048,352]{1,2,0:T(8,128)(2,1)S(1)} %fusion.1) | data formatting | bytes 2883584 | tf_op jit(solution)/shard_map/convert_element_type | solution.py:56
  42.0 0.5 broadcast.53
  42.5 34.4 %reduce = bf16[2048,352]{1,0:T(8,128)(2,1)S(1)} reduce(bf16[2048,1,352]{2,1,0:T(2,128)(2,1)} %bitcast.16, bf16[]{:T(256)} %broadcast.53), dimensions={1}, to_apply=%bitcast.7.reduce_sub_computation | reduce | bytes 2883586
  76.9 3.6 %reshape.41 = bf16[4,2,90112]{2,1,0:T(2,128)(2,1)} reshape(bf16[2048,352]{1,0:T(8,128)(2,1)S(1)} %reduce) | data formatting | bytes 2883584
  80.5 4.9 %all-to-all-start = ((bf16[4,2,90112]{2,1,0:T(2,128)(2,1)}), bf16[4,2,90112]{2,1,0:T(2,128)(2,1)S(1)}, u32[]{:S(2)}, u32[]{:S(2)}) async-start(bf16[4,2,90112]{2,1,0:T(2,128)(2,1)} %reshape.41), calls=%async_computation.1 | async-start | bytes 2883584 | tf_op jit(solution)/shard_map/all_to_all | solution.py:55
  85.4 1.1 convert_multiply_fusion
  86.5 1.1 multiply_reduce_fusion
  87.6 51.7 %psum.7 = f32[2048]{0:T(1024)} all-reduce(f32[2048]{0:T(1024)S(1)} %get-tuple-element.3), channel_id=1, replica_groups=mesh['rep'=4,'fs'=4,'tp'=2] {'rep','fs','tp'}, use_global_device_ids=true, to_apply=%region_4.0 | all-reduce | flops 2048 | bytes 16384 | tf_op jit(solution)/shard_map/psum | solution.py:48
  139.4 1.7 %multiply_convert_fusion.6 = bf16[16,2048]{1,0:T(8,128)(2,1)} fusion(f32[16,2048]{1,0:T(8,128)} %reduce-scatter.2.cloned.1.call-done, f32[128,2048]{1,0:T(8,128)} %convert_multiply_fusion, s32[]{:T(128)S(6)} %select_n.4, f32[16]{0:T(128)S(1)} %broadcast_multiply_fusion, f32[2048]{0:T(1024)S(1)} %copy-done.7, f32[16]{0:T(128)S(1)} %dynamic-slice.3), kind=kLoop, calls=%fused_computation.17 | loop fusion | flops 163840 | bytes 336004 | tf_op jit(solution)/shard_map/convert_element_type | solution.py:52
  141.1 4.0 %reshape.42 = bf16[2048,1,352]{2,1,0:T(2,128)(2,1)} reshape(bf16[4,2,90112]{2,1,0:T(2,128)(2,1)S(1)} %all-to-all-done) | data formatting | bytes 2883584
  145.0 7.0 %copy.13 = bf16[1,2048,352]{1,2,0:T(8,128)(2,1)S(1)} copy(bf16[1,2048,352]{2,0,1:T(2,128)(2,1)} %bitcast.17) | data formatting | bytes 2883584 | tf_op jit(solution)/shard_map/all_to_all | solution.py:55
  152.0 3.4 %reshape.40 = f32[4,512,352]{1,0,2:T(4,128)} reshape(bf16[1,2048,352]{1,2,0:T(8,128)(2,1)S(1)} %copy.13) | data formatting | bytes 4325376 | tf_op jit(solution)/shard_map/convert_element_type | solution.py:57
  155.5 4.4 %reduce_sum.39 = f32[512,352]{0,1:T(8,128)} reduce(f32[4,512,352]{1,0,2:T(4,128)} %reshape.40, f32[]{:T(128)} %constant.11.clone.1), dimensions={0}, to_apply=%region_5.0 | reduce | flops 540672 | bytes 3604484 | tf_op jit(solution)/shard_map/reduce_sum | solution.py:58
  (21 shorter events, 0.2 us)
Async XLA Ops:
  7.2 12.0 %copy-start = (bf16[2048,352]{0,1:T(8,128)(2,1)S(1)}, bf16[2048,352]{0,1:T(8,128)(2,1)}, u32[]{:S(2)}) copy-start(bf16[2048,352]{0,1:T(8,128)(2,1)} %param.9) | copy-start | bytes 4325380
  7.2 79.3 %reduce-scatter.2.cloned.1.call-start = ((), (), s32[]{:S(2)}) async-start(), calls=%async_computation.2 | async-start | bytes 1179648 | tf_op jit(solution)/shard_map/reduce_scatter | solution.py:39
  19.0 1.6 copy-start.4
  19.0 1.6 copy-start.7
  20.6 12.3 %copy-start.2 = (f32[128,352]{0,1:T(8,128)}, f32[128,352]{0,1:T(8,128)S(1)}, u32[]{:S(2)}) copy-start(f32[128,352]{0,1:T(8,128)S(1)} %fusion.3) | copy-start | bytes 540676
  20.6 0.9 copy-start.6
  20.7 11.2 %copy-start.3 = (bf16[352,2048]{1,0:T(8,128)(2,1)S(1)}, bf16[352,2048]{1,0:T(8,128)(2,1)}, u32[]{:S(2)}) copy-start(bf16[352,2048]{1,0:T(8,128)(2,1)} %param.11) | copy-start | bytes 4325380
  21.6 11.4 %copy-start.5 = (f32[128,352]{0,1:T(8,128)}, f32[128,352]{0,1:T(8,128)S(1)}, u32[]{:S(2)}) copy-start(f32[128,352]{0,1:T(8,128)S(1)} %fusion.4) | copy-start | bytes 540676
  31.1 0.8 copy-start.1
  80.5 60.6 %all-to-all-start = ((bf16[4,2,90112]{2,1,0:T(2,128)(2,1)}), bf16[4,2,90112]{2,1,0:T(2,128)(2,1)S(1)}, u32[]{:S(2)}, u32[]{:S(2)}) async-start(bf16[4,2,90112]{2,1,0:T(2,128)(2,1)} %reshape.41), calls=%async_computation.1 | async-start | bytes 2883584 | tf_op jit(solution)/shard_map/all_to_all | solution.py:55
Sparse Core Ops, SparseCore 0:
  34.6 36.2 reduce-scatter.1
where the time goes:
time: 167 us
  blocking collectives  73 us (44%)
  other arithmetic  42.9 us (26%)
  local copies, waits for them, and re-layouts  25.4 us (15%)
  between operations  14.2 us (9%)
  matrix products  6.35 us (4%)
  starting transfers between devices  4.91 us (3%)
    psum x1, blocking collectives, per_device(): lax.psum(jnp.sum(d_in * own_normed, axis=0), ('rep', 'fs', 'tp'))  51.7 us
    unnamed x1, other arithmetic  34.4 us
    all_gather x1, blocking collectives, per_device(): lax.all_gather(inputs, ('fs', 'tp'), axis=0, tiled=True)  11.8 us
    all_gather x1, blocking collectives, per_device(): lax.all_gather(cotangent, ('fs', 'tp'), axis=0, tiled=True)  9.52 us
    unnamed x19, local copies, waits for them, and re-layouts  9.19 us
    all_to_all x1, local copies, waits for them, and re-layouts, per_device(): lax.all_to_all(part_down[None].astype(jnp.bfloat16), 'rep', split_axis=1,...  7.01 us
    convert_element_type x1, local copies, waits for them, and re-layouts, per_device(): part_down[None].astype(jnp.bfloat16)  5.72 us
    all_to_all x1, starting transfers between devices, per_device(): lax.all_to_all(part_down[None].astype(jnp.bfloat16), 'rep', split_axis=1,...  4.87 us
  transfers between devices with their start and end apart: 2, of which 0 were waited for; matrix products, arithmetic and copies ran while one was open for 30% of the time, Pallas kernels for 0%

commit v1 on v0

--- a/solution.py
+++ b/solution.py
@@ -52,8 +52,16 @@
     ).astype(jnp.bfloat16)
     input_grad, gain_grad = (input_grad, gain_grad)
     part_down = 0.5 * across_tokens(whole_dy, hidden)
-    got_down = lax.all_to_all(
-        part_down[None].astype(jnp.bfloat16), "rep", split_axis=1, concat_axis=0, tiled=True
+    got_down = jnp.concatenate(
+        lax.all_to_all(
+            jnp.stack(
+                jnp.split(part_down[None].astype(jnp.bfloat16), lax.axis_size("rep"), axis=1)
+            ),
+            "rep",
+            0,
+            0,
+        ),
+        axis=0,
     ).astype(jnp.float32)
     down_grad = jnp.sum(got_down, axis=0).T
     return (input_grad, gain_grad, down_grad)

time: 167 us -> 120 us (0.72)
  other arithmetic: 42.9 us -> 6.47 us
  waiting for transfers between devices: 0.02 us -> 28.4 us
  local copies, waits for them, and re-layouts: 25.4 us -> 0.95 us
  blocking collectives: 73 us -> 60.8 us
  matrix products: 6.35 us -> 4.33 us
    unnamed x1 -> x0, other arithmetic: 34.4 us -> none
    reduce_scatter x1, waiting for transfers between devices: 0.01 us -> 28.4 us  [per_device(): lax.psum_scatter(across_columns(d_gate, gate_weight) + across_columns(d_u...]
    psum x1, blocking collectives: 51.7 us -> 39.4 us  [per_device(): lax.psum(jnp.sum(d_in * own_normed, axis=0), ('rep', 'fs', 'tp'))]
    convert_element_type x2 -> x0, local copies, waits for them, and re-layouts: 9.15 us -> none  [the longest x1 5.72 us: per_device(): part_down[None].astype(jnp.bfloat16)]
    unnamed x19 -> x8, local copies, waits for them, and re-layouts: 9.19 us -> 0.75 us
    all_to_all x1 -> x0, local copies, waits for them, and re-layouts: 7.01 us -> none  [per_device(): lax.all_to_all(part_down[None].astype(jnp.bfloat16), 'rep', split_axis=1,...]
    reduce_sum x1, other arithmetic: 4.38 us -> 1.07 us  [per_device(): down_grad = jnp.sum(got_down, axis=0).T]
  transfers between devices with their start and end apart: 2 -> 2, of which waited for: 0 -> 1; matrix products, arithmetic and copies ran while one was open for 30% -> 5% of each run, Pallas kernels for 0% -> 0%
where the time goes in v1:
time: 120 us
  blocking collectives  60.8 us (51%)
  waiting for transfers between devices  28.4 us (24%)
  between operations  14.1 us (12%)
  other arithmetic  6.47 us (5%)
  starting transfers between devices  4.88 us (4%)
  matrix products  4.33 us (4%)
    psum x1, blocking collectives, per_device(): lax.psum(jnp.sum(d_in * own_normed, axis=0), ('rep', 'fs', 'tp'))  39.4 us
    reduce_scatter x1, waiting for transfers between devices, per_device(): lax.psum_scatter(across_columns(d_gate, gate_weight) + across_columns(d_u...  28.4 us
    all_gather x1, blocking collectives, per_device(): lax.all_gather(inputs, ('fs', 'tp'), axis=0, tiled=True)  11.8 us
    all_gather x1, blocking collectives, per_device(): lax.all_gather(cotangent, ('fs', 'tp'), axis=0, tiled=True)  9.67 us
    all_to_all x1, starting transfers between devices, per_device(): lax.all_to_all(jnp.stack(jnp.split(part_down[None].astype(jnp.bfloat16),...  4.85 us
    dot_general x3, matrix products, across_columns(): lax.dot_general(left, right, (((1,), (1,)), ((), ())), preferred_element_...  2.56 us
  transfers between devices with their start and end apart: 2, of which 1 were waited for; matrix products, arithmetic and copies ran while one was open for 5% of the time, Pallas kernels for 0%

profile of v1, /device:TPU:0, one launch (start us, length us, event | category | flops | bytes accessed | tf_op | source)
XLA Modules:
  0.0 119.9 jit_solution(9823612420348382070)
XLA Ops:
  7.2 0.0 copy-start
  7.2 0.0 reduce-scatter.2.cloned.1.call-start
  7.2 11.8 %all_gather.6 = bf16[128,2048]{1,0:T(8,128)(2,1)S(1)} all-gather(bf16[16,2048]{1,0:T(8,128)(2,1)} %param.6), channel_id=1, replica_groups=mesh['rep'=4,'fs'=4,'tp'=2] {'fs','tp'}, dimensions={0}, use_global_device_ids=true | all-gather | bytes 589824 | tf_op jit(solution)/shard_map/all_gather | solution.py:23
  19.0 0.2 fusion.2
  19.2 9.7 %all_gather.7 = bf16[128,2048]{1,0:T(8,128)(2,1)S(1)} all-gather(bf16[16,2048]{1,0:T(8,128)(2,1)} %param.7), channel_id=1, replica_groups=mesh['rep'=4,'fs'=4,'tp'=2] {'fs','tp'}, dimensions={0}, use_global_device_ids=true | all-gather | bytes 589824 | tf_op jit(solution)/shard_map/all_gather | solution.py:24
  28.9 0.6 fusion.3
  29.5 0.0 copy-start.1
  29.5 0.6 fusion.4
  30.1 0.7 copy-done.1
  30.9 0.5 convolution_multiply_fusion.1
  31.4 0.5 fusion.6
  32.0 1.5 %convolution_add_fusion = f32[128,2048]{1,0:T(8,128)} fusion(f32[128,2048]{1,0:T(8,128)S(1)} %fusion.6, bf16[2048,352]{0,1:T(8,128)(2,1)S(1)} %copy-done.2, f32[128,352]{0,1:T(8,128)S(1)} %convolution_multiply_fusion.1, f32[128,352]{0,1:T(8,128)S(1)} %fusion.3), kind=kOutput, calls=%fused_computation.4 | convolution fusion | flops 185081856 | bytes 3899392 | tf_op jit(solution)/shard_map/dot_general | solution.py:16
  33.4 0.0 reduce-scatter.2.cloned.1.call-update
  33.5 0.5 fusion.1
  34.0 0.1 slice_bitcast_fusion.3
  34.1 1.3 %pad_maximum_fusion = bf16[4,1,512,352]{2,3,1,0:T(8,128)(2,1)} fusion(bf16[1,1,512,352]{2,3,1,0:T(8,128)(2,1)S(1)} %get-tuple-element.6, bf16[1,1,512,352]{2,3,1,0:T(8,128)(2,1)S(1)} %get-tuple-element.7, bf16[1,1,512,352]{2,3,1,0:T(8,128)(2,1)S(1)} %get-tuple-element.8, bf16[1,1,512,352]{2,3,1,0:T(8,128)(2,1)S(1)} %get-tuple-element.5), kind=kLoop, calls=%fused_computation.5 | loop fusion | flops 2162688 | bytes 2883584 | tf_op jit(solution)/shard_map/stack | solution.py:57
  35.4 4.8 %all-to-all-start = ((bf16[4,1,512,352]{2,3,1,0:T(8,128)(2,1)}), bf16[4,1,512,352]{2,3,1,0:T(8,128)(2,1)S(1)}, u32[]{:S(2)}, u32[]{:S(2)}) async-start(bf16[4,1,512,352]{2,3,1,0:T(8,128)(2,1)} %pad_maximum_fusion), calls=%async_computation.1 | async-start | bytes 2883584 | tf_op jit(solution)/shard_map/all_to_all | solution.py:56
  40.3 0.1 dynamic-slice.3
  40.4 1.1 convert_multiply_fusion
  41.5 28.4 %reduce-scatter.2.cloned.1.call-done = f32[16,2048]{1,0:T(8,128)} async-done(((f32[128,2048]{1,0:T(8,128)}), f32[16,2048]{1,0:T(8,128)}) %reduce-scatter.2.cloned.1.call-update) | async-done | bytes 131088 | tf_op jit(solution)/shard_map/reduce_scatter | solution.py:39
  69.8 1.1 multiply_reduce_fusion
  71.0 39.4 %psum.7 = f32[2048]{0:T(1024)} all-reduce(f32[2048]{0:T(1024)S(1)} %get-tuple-element.3), channel_id=1, replica_groups=mesh['rep'=4,'fs'=4,'tp'=2] {'rep','fs','tp'}, use_global_device_ids=true, to_apply=%region_4.0 | all-reduce | flops 2048 | bytes 16384 | tf_op jit(solution)/shard_map/psum | solution.py:48
  110.3 1.7 %multiply_convert_fusion.6 = bf16[16,2048]{1,0:T(8,128)(2,1)} fusion(f32[16,2048]{1,0:T(8,128)} %reduce-scatter.2.cloned.1.call-done, f32[128,2048]{1,0:T(8,128)} %convert_multiply_fusion, s32[]{:T(128)S(6)} %select_n.4, f32[16]{0:T(128)S(1)} %broadcast_multiply_fusion, f32[2048]{0:T(1024)S(1)} %copy-done.3, f32[16]{0:T(128)S(1)} %dynamic-slice.3), kind=kLoop, calls=%fused_computation.23 | loop fusion | flops 163840 | bytes 336004 | tf_op jit(solution)/shard_map/convert_element_type | solution.py:52
  112.0 1.1 convert_reduce_fusion
  (8 shorter events, 0.0 us)
Async XLA Ops:
  7.2 21.7 %copy-start = (bf16[2048,352]{0,1:T(8,128)(2,1)S(1)}, bf16[2048,352]{0,1:T(8,128)(2,1)}, u32[]{:S(2)}) copy-start(bf16[2048,352]{0,1:T(8,128)(2,1)} %param.9) | copy-start | bytes 4325380
  7.2 21.7 %copy-start.3 = (f32[2048]{0:T(1024)S(1)}, f32[2048]{0:T(1024)}, u32[]{:S(2)}) copy-start(f32[2048]{0:T(1024)} %param.8) | copy-start | bytes 24580
  7.2 62.6 %reduce-scatter.2.cloned.1.call-start = ((), (), s32[]{:S(2)}) async-start(), calls=%async_computation.2 | async-start | bytes 1179648 | tf_op jit(solution)/shard_map/reduce_scatter | solution.py:39
  19.2 10.3 %copy-start.2 = (bf16[2048,352]{0,1:T(8,128)(2,1)S(1)}, bf16[2048,352]{0,1:T(8,128)(2,1)}, u32[]{:S(2)}) copy-start(bf16[2048,352]{0,1:T(8,128)(2,1)} %param.10) | copy-start | bytes 4325380
  29.5 1.4 %copy-start.1 = (bf16[352,2048]{1,0:T(8,128)(2,1)S(1)}, bf16[352,2048]{1,0:T(8,128)(2,1)}, u32[]{:S(2)}) copy-start(bf16[352,2048]{1,0:T(8,128)(2,1)} %param.11) | copy-start | bytes 4325380
  35.4 76.5 %all-to-all-start = ((bf16[4,1,512,352]{2,3,1,0:T(8,128)(2,1)}), bf16[4,1,512,352]{2,3,1,0:T(8,128)(2,1)S(1)}, u32[]{:S(2)}, u32[]{:S(2)}) async-start(bf16[4,1,512,352]{2,3,1,0:T(8,128)(2,1)} %pad_maximum_fusion), calls=%async_computation.1 | async-start | bytes 2883584 | tf_op jit(solution)/shard_map/all_to_all | solution.py:56
Sparse Core Ops, SparseCore 0:
  33.6 36.2 reduce-scatter.1
